TPU v7x, 256 devices: a whole 4x4x8 slice. The times are simulated.
256 devices in a mesh: ep: 64 (over z, y, core), tp: 4 (over x).
Axes of the slice: x: 4, y: 4, z: 8, core: 2. Of those that a mesh axis runs over, the one named last changes fastest.
Arguments:
- mixer_in: bfloat16 [24576, 2048], P(('ep', 'tp')), may hold values from -6 to 6
- expert_in: bfloat16 [24576, 2048], P(('ep', 'tp')), may hold values from -6 to 6
- mixer_gain: float32 [2048], replicated, may hold values from 0.1 to 1.9
- in_gate_weight: bfloat16 [2048, 2048], P(None, 'tp'), may hold values from -0.125 to 0.125
- out_gate_weight: bfloat16 [2048, 2048], P(None, 'tp'), may hold values from -0.125 to 0.125
- value_weight: bfloat16 [2048, 2048], P(None, 'tp'), may hold values from -0.125 to 0.125
- conv_taps: float32 [3, 2048], replicated, may hold values from -3 to 3
- mixer_proj: bfloat16 [2048, 2048], P(None, 'tp'), may hold values from -0.125 to 0.125
- expert_gain: float32 [2048], replicated, may hold values from 0.1 to 1.9
- route_ids: int32 [24576, 2], P('ep'), may hold values from 0 to 63, all different within a row; in each aligned block of 96 rows (0 to 95, 96 to 191, ...) at most 6 rows name the same one
- route_weights: float32 [24576, 2], P('ep'), may hold values from 0.1 to 1
- gate_weight: bfloat16 [64, 2048, 1024], P('ep', None, 'tp'), may hold values from -0.125 to 0.125
- up_weight: bfloat16 [64, 2048, 1024], P('ep', None, 'tp'), may hold values from -0.125 to 0.125
- down_weight: bfloat16 [64, 1024, 2048], P('ep', None, 'tp'), may hold values from -0.1875 to 0.1875
Outputs:
- mixer_out: bfloat16 [24576, 2048], P('ep', 'tp')
- expert_out: bfloat16 [24576, 2048], P('ep', 'tp')
Inputs may be any that keep to these rules, and one draw needn't show every extreme that they name: `route_ids`: each row names 2 different experts. In each aligned block of 96 rows no expert is named by more than 6 rows, a bound that some block reaches.
All inputs are finite; a program needn't handle non-finite values.
Results may differ from a plain program's by a relative error of at most 0.0076.
Values may be sent and summed in bfloat16 or wider, within the bound.
A program may use at most 64 MiB of HBM per device.

v0:
```python
import jax
import jax.numpy as jnp
from jax import lax
from jax.sharding import PartitionSpec as P

norm_eps = 1e-06


def sent_to_all(x, axis):
    peers = lax.axis_size(axis)
    return lax.all_to_all(jnp.broadcast_to(x[None], (peers, *x.shape)), axis, 0, 0, tiled=True)


def joined_along(tiles, dim):
    tiles = jnp.moveaxis(tiles, 0, dim)
    dims = tiles.shape
    return tiles.reshape(*dims[:dim], dims[dim] * dims[dim + 1], *dims[dim + 2 :])


def collect(x, axis, dim):
    tiles = sent_to_all(x, axis)
    return joined_along(tiles, dim)


def passed_along(value, axis, steps):
    count = lax.axis_size(axis)
    leading, last = (max(0, -steps), min(count, count - steps))
    return lax.ppermute(value, axis, [(source, source + steps) for source in range(leading, last)])


def rms_rows(values, gain_row):
    wide = values.astype(jnp.float32)
    scale = lax.rsqrt(jnp.mean(wide * wide, axis=-1, keepdims=True) + norm_eps)
    return (wide * scale * gain_row).astype(jnp.bfloat16)


def place_slots(route_ids, group_rows, experts, slot_cap):
    row_total, top_count = route_ids.shape
    groups = row_total // group_rows
    labels = jnp.arange(experts, dtype=jnp.int32)
    onehot = (
        route_ids.reshape(groups, group_rows * top_count)[:, :, None] == labels[None, None, :]
    ).astype(jnp.int32)
    earlier = jnp.cumsum(onehot, axis=1) - onehot
    within = jnp.sum(earlier * onehot, axis=2)
    slot_index = jnp.arange(groups, dtype=jnp.int32)[:, None] * slot_cap + within
    return slot_index.reshape(row_total, top_count)


def on_device(
    mixer_in,
    expert_in,
    mixer_gain,
    in_gate_weight,
    out_gate_weight,
    value_weight,
    conv_taps,
    mixer_proj,
    expert_gain,
    route_ids,
    route_weights,
    gate_weight,
    up_weight,
    down_weight,
):
    tok_dev = mixer_in.shape[0]
    tp_count = lax.axis_size("tp")
    ep_count = lax.axis_size("ep")
    top_count = route_ids.shape[1]
    experts = ep_count * gate_weight.shape[0]
    slot_cap = max(2, 2 * tok_dev * top_count // experts)
    tp_index = lax.axis_index("tp")
    mixer_normed = rms_rows(mixer_in, mixer_gain)
    expert_normed = rms_rows(expert_in, expert_gain)
    block_slot = place_slots(route_ids, tok_dev, experts, slot_cap)
    mixer_rows = collect(mixer_normed, "tp", 0)
    send_ids = lax.dynamic_slice_in_dim(route_ids, tp_index * tok_dev, tok_dev, 0)
    send_slot = (
        lax.dynamic_slice_in_dim(block_slot, tp_index * tok_dev, tok_dev, 0) - tp_index * slot_cap
    )
    source_count = expert_normed.shape[0]
    flat_index = (send_ids * slot_cap + send_slot).reshape(-1)
    row_table = (
        jnp.full((experts * slot_cap,), source_count, jnp.int32)
        .at[flat_index]
        .set(jnp.repeat(jnp.arange(source_count, dtype=jnp.int32), top_count))
    )
    padded_rows = jnp.concatenate(
        [expert_normed, jnp.zeros((1, expert_normed.shape[1]), jnp.bfloat16)], axis=0
    )
    outgoing = padded_rows[row_table].reshape(experts, slot_cap, expert_normed.shape[1])
    arrived = lax.all_to_all(outgoing, "ep", split_axis=0, concat_axis=0, tiled=True)
    arrived = lax.all_gather(arrived, "tp", axis=1, tiled=True)
    chan_width = in_gate_weight.shape[1]
    in_gate = jnp.dot(mixer_rows, in_gate_weight, preferred_element_type=jnp.float32)
    out_gate = jnp.dot(mixer_rows, out_gate_weight, preferred_element_type=jnp.float32)
    values = jnp.dot(mixer_rows, value_weight, preferred_element_type=jnp.float32)
    product = (in_gate * values).astype(jnp.bfloat16)
    tap_count = conv_taps.shape[0]
    rim_rows = passed_along(product[product.shape[0] - (tap_count - 1) :], "ep", 1)
    extended = jnp.concatenate([rim_rows, product], axis=0).astype(jnp.float32)
    tap_rows = lax.dynamic_slice_in_dim(conv_taps, tp_index * chan_width, chan_width, 1)
    row_count = product.shape[0]
    conv_sum = tap_rows[0] * extended[0:row_count]
    for tap_index in range(1, tap_count):
        conv_sum = conv_sum + tap_rows[tap_index] * extended[tap_index : tap_index + row_count]
    gated = (out_gate * conv_sum).astype(jnp.bfloat16)
    slots_in = arrived.reshape(-1, arrived.shape[2])
    gate_pre = jnp.dot(slots_in, gate_weight[0], preferred_element_type=jnp.float32)
    up_pre = jnp.dot(slots_in, up_weight[0], preferred_element_type=jnp.float32)
    hidden = (jax.nn.silu(gate_pre) * up_pre).astype(jnp.bfloat16)
    down_slice = down_weight[0]
    rows_part = mixer_proj
    mixer_sum = jnp.dot(
        lax.all_gather(gated, "tp", axis=1, tiled=True),
        rows_part,
        preferred_element_type=jnp.float32,
    )
    rows_part = down_slice
    expert_sum = jnp.dot(
        lax.all_gather(hidden, "tp", axis=1, tiled=True),
        rows_part,
        preferred_element_type=jnp.float32,
    )
    mixer_out = mixer_sum.astype(jnp.bfloat16)
    results = expert_sum.astype(jnp.bfloat16).reshape(ep_count, -1, expert_sum.shape[1])
    returned = lax.all_to_all(results, "ep", split_axis=0, concat_axis=0, tiled=True)
    back_index = (route_ids * (tp_count * slot_cap) + block_slot).reshape(-1)
    picked = returned.reshape(-1, returned.shape[2])[back_index].reshape(
        route_ids.shape[0], top_count, -1
    )
    shares = route_weights / jnp.sum(route_weights, axis=1, keepdims=True)
    expert_out = jnp.sum(picked.astype(jnp.float32) * shares[:, :, None], axis=1).astype(
        jnp.bfloat16
    )
    return (mixer_out, expert_out)


def solution(mesh):
    return jax.shard_map(
        on_device,
        mesh=mesh,
        in_specs=(
            P(("ep", "tp"), None),
            P(("ep", "tp"), None),
            P(),
            P(None, "tp"),
            P(None, "tp"),
            P(None, "tp"),
            P(),
            P(None, "tp"),
            P(),
            P("ep", None),
            P("ep", None),
            P("ep", None, "tp"),
            P("ep", None, "tp"),
            P("ep", None, "tp"),
        ),
        out_specs=(P("ep", "tp"), P("ep", "tp")),
        check_vma=False,
    )
```

profile of v0, /device:TPU:1, one launch (start us, length us, event | category | flops | bytes accessed | tf_op | source)
XLA Modules:
  0.0 291.8 jit_solution(16893624878074087516)
XLA Ops:
  7.2 1.0 copy.47
  8.5 2.4 reduce-window.6
  12.3 1.2 scatter_custom_fusion
  13.6 0.2 fusion.10
  14.0 3.1 %gather_fusion = bf16[384,2048]{1,0:T(8,128)(2,1)} fusion(bf16[97,2048]{1,0:T(8,128)(2,1)S(1)} %concatenate.7, s32[1024]{0:T(1024)S(1)} %pad_clamp_fusion.1), kind=kCustom, calls=%fused_computation | custom fusion | bytes 3147264 | tf_op jit(solution)/shard_map/gather | solution.py:91
  17.1 3.7 %reshape.133 = bf16[64,6,2048]{2,1,0:T(8,128)(2,1)} reshape(bf16[384,2048]{1,0:T(8,128)(2,1)} %gather_fusion) | data formatting | bytes 3145728 | tf_op jit(solution)/shard_map/reshape | solution.py:91
  20.8 62.8 %all_to_all.15 = bf16[64,6,2048]{2,1,0:T(8,128)(2,1)S(1)} all-to-all(bf16[64,6,2048]{2,1,0:T(8,128)(2,1)} %reshape.133), channel_id=1, replica_groups=mesh['ep'=64,'tp'=4] {'ep'}, dimensions={0} | all-to-all | bytes 3145728 | tf_op jit(solution)/shard_map/all_to_all | solution.py:92
  83.6 2.0 copy.54
  85.7 0.2 all-gather.8.cloned.1.call-start
  85.9 65.5 %all-gather.6.cloned.1.call-done = bf16[64,24,2048]{2,0,1:T(8,128)(2,1)} async-done(((bf16[64,6,2048]{2,0,1:T(8,128)(2,1)}), bf16[64,24,2048]{2,0,1:T(8,128)(2,1)}) %all-gather.6.cloned.1.call-update) | async-done | bytes 6291472 | tf_op jit(solution)/shard_map/all_gather | solution.py:93
  151.4 6.2 %copy.55 = bf16[64,24,2048]{2,1,0:T(8,128)(2,1)S(1)} copy(bf16[64,24,2048]{2,0,1:T(8,128)(2,1)} %all-gather.6.cloned.1.call-done) | data formatting | bytes 12582912 | tf_op jit(solution)/shard_map/all_gather | solution.py:93
  157.7 3.2 %fusion.5 = f32[1536,256]{1,0:T(8,128)S(1)} fusion(bf16[1536,2048]{1,0:T(8,128)(2,1)S(1)} %bitcast.43, bf16[1,2048,256]{2,1,0:T(8,128)(2,1)} %param.25), kind=kOutput, calls=%fused_computation.14 | convolution fusion | flops 1610612736 | bytes 8912896 | tf_op jit(solution)/shard_map/dot_general | solution.py:109
  160.9 3.0 %fusion = bf16[1536,256]{1,0:T(8,128)(2,1)} fusion(bf16[1536,2048]{1,0:T(8,128)(2,1)S(1)} %bitcast.44, f32[1536,256]{1,0:T(8,128)S(1)} %fusion.5, bf16[1,2048,256]{2,1,0:T(8,128)(2,1)S(1)} %copy-done.8), kind=kOutput, calls=%fused_computation.5 | convolution fusion | flops 1612972032 | bytes 9699328 | tf_op jit(solution)/shard_map/dot_general | solution.py:110
  163.9 0.2 fusion.7
  164.3 1.4 broadcast_in_dim.8
  165.6 4.3 %all-to-all-start = ((bf16[4,96,2048]{2,1,0:T(8,128)(2,1)}), bf16[4,96,2048]{2,1,0:T(8,128)(2,1)}, u32[]{:S(2)}, u32[]{:S(2)}) async-start(bf16[4,96,2048]{2,1,0:T(8,128)(2,1)} %broadcast_in_dim.8), calls=%async_computation | async-start | bytes 3145728 | tf_op jit(solution)/shard_map/all_to_all | solution.py:11
  170.0 28.0 %all-to-all-done = bf16[4,96,2048]{2,1,0:T(8,128)(2,1)} async-done(((bf16[4,96,2048]{2,1,0:T(8,128)(2,1)}), bf16[4,96,2048]{2,1,0:T(8,128)(2,1)}, u32[]{:S(2)}, u32[]{:S(2)}) %all-to-all-start) | async-done | bytes 1572896 | tf_op jit(solution)/shard_map/all_to_all | solution.py:11
  198.0 2.5 fusion.22
  200.6 2.4 fusion.2
  203.0 5.1 %collective-permute-start = (bf16[2,512]{1,0:T(2,128)(2,1)S(1)}, bf16[2,512]{1,0:T(2,128)(2,1)S(1)}, u32[]{:S(2)}, u32[]{:S(2)}) collective-permute-start(bf16[2,512]{1,0:T(2,128)(2,1)S(1)} %slice.44), channel_id=1, source_target_pairs={{0,4},{4,8},{8,12},{12,16},{16,20},{20,24},{24,28},{28,32},{32,36}... | collective-permute-start | bytes 6152 | tf_op jit(solution)/shard_map/ppermute | solution.py:28
  208.2 0.9 constant_dynamic-slice_fusion
  209.2 8.7 %all-gather.8.cloned.1.call-done = bf16[1536,1024]{1,0:T(8,128)(2,1)} async-done(((bf16[1536,256]{1,0:T(8,128)(2,1)}), bf16[1536,1024]{1,0:T(8,128)(2,1)}) %all-gather.8.cloned.1.call-update) | async-done | bytes 3145744 | tf_op jit(solution)/shard_map/all_gather | solution.py:121
  217.8 5.1 %convolution_convert_fusion = bf16[1536,512]{1,0:T(8,128)(2,1)} fusion(bf16[1536,1024]{1,0:T(8,128)(2,1)} %all-gather.8.cloned.1.call-done, bf16[1,1024,512]{2,1,0:T(8,128)(2,1)} %param.27), kind=kOutput, calls=%fused_computation.3 | convolution fusion | flops 1611399168 | bytes 5767168 | tf_op jit(solution)/shard_map/dot_general | solution.py:120
  223.0 12.5 %all-to-all-start.2 = ((bf16[64,24,512]{2,1,0:T(8,128)(2,1)}), bf16[64,24,512]{2,1,0:T(8,128)(2,1)}, u32[]{:S(2)}, u32[]{:S(2)}) async-start(bf16[64,24,512]{2,1,0:T(8,128)(2,1)} %bitcast.45), calls=%async_computation.2 | async-start | bytes 3145728 | tf_op jit(solution)/shard_map/all_to_all | solution.py:127
  235.5 0.3 all-gather.4.cloned.1.call-start
  235.7 3.9 %fusion.1 = bf16[384,512]{1,0:T(8,128)(2,1)} fusion(bf16[384,2048]{1,0:T(8,128)(2,1)} %bitcast, bf16[2048,512]{1,0:T(8,128)(2,1)} %param.18, f32[386,512]{1,0:T(8,128)S(1)} %maximum_convert_fusion, f32[512]{0:T(512)S(1)} %bitcast.48, f32[512]{0:T(512)S(1)} %bitcast.47, f32[512]{0:T(512)S(1)} %bitcast.46), kind=kOutput, calls=%fused_computation.9 | convolution fusion | flops 806682624 | bytes 6428672 | tf_op jit(solution)/shard_map/dot_general | solution.py:96
  240.2 28.4 %all-gather.4.cloned.1.call-done = bf16[384,2048]{1,0:T(8,128)(2,1)} async-done(((bf16[384,512]{1,0:T(8,128)(2,1)}), bf16[384,2048]{1,0:T(8,128)(2,1)}) %all-gather.4.cloned.1.call-update) | async-done | bytes 1572880 | tf_op jit(solution)/shard_map/all_gather | solution.py:115
  268.6 3.8 %convolution_convert_fusion.1 = bf16[384,512]{1,0:T(8,128)(2,1)} fusion(bf16[384,2048]{1,0:T(8,128)(2,1)} %all-gather.4.cloned.1.call-done, bf16[2048,512]{1,0:T(8,128)(2,1)} %param.21), kind=kOutput, calls=%fused_computation.11 | convolution fusion | flops 805502976 | bytes 4063232 | tf_op jit(solution)/shard_map/dot_general | solution.py:114
  272.4 2.1 all-to-all-done.2
  274.5 4.3 %gather_fusion.1 = bf16[768,512]{1,0:T(8,128)(2,1)S(1)} fusion(bf16[1536,512]{1,0:T(8,128)(2,1)} %bitcast.12, s32[1024]{0:T(1024)S(1)} %pad_clamp_fusion), kind=kCustom, calls=%fused_computation.1 | custom fusion | bytes 1575936 | tf_op jit(solution)/shard_map/gather | solution.py:129
  278.8 2.1 reshape.139
  280.9 4.3 %multiply_reduce_fusion = bf16[384,512]{1,0:T(8,128)(2,1)} fusion(f32[384,2,512]{2,1,0:T(2,128)} %reshape.139, f32[384,2]{1,0:T(8,128)S(1)} %copy.57), kind=kLoop, calls=%fused_computation.6 | loop fusion | flops 589824 | bytes 1969152 | tf_op jit(solution)/shard_map/reduce_sum | solution.py:133
  (61 shorter events, 2.8 us)
Async XLA Ops:
  7.2 190.8 %copy-start = (bf16[2048,512]{1,0:T(8,128)(2,1)S(1)}, bf16[2048,512]{1,0:T(8,128)(2,1)}, u32[]{:S(2)}) copy-start(bf16[2048,512]{1,0:T(8,128)(2,1)} %param.17) | copy-start | bytes 6291460
  7.2 144.2 %all-gather.6.cloned.1.call-start = ((), (), s32[]{:S(2)}) async-start(), calls=%async_computation.4 | async-start | bytes 7864320 | tf_op jit(solution)/shard_map/all_gather | solution.py:93
  8.2 3.6 %copy-start.3 = (s32[384,2]{0,1:T(2,128)S(1)}, s32[384,2]{0,1:T(2,128)}, u32[]{:S(2)}) copy-start(s32[384,2]{0,1:T(2,128)} %param.23) | copy-start | bytes 9220
  8.4 5.1 %copy-start.1 = (bf16[96,2048]{1,0:T(8,128)(2,1)S(1)}, bf16[96,2048]{1,0:T(8,128)(2,1)}, u32[]{:S(2)}) copy-start(bf16[96,2048]{1,0:T(8,128)(2,1)} %param.15) | copy-start | bytes 1179652
  8.5 5.3 %copy-start.5 = (f32[2048]{0:T(1024)S(1)}, f32[2048]{0:T(1024)}, u32[]{:S(2)}) copy-start(f32[2048]{0:T(1024)} %param.22) | copy-start | bytes 24580
  85.7 132.2 %all-gather.8.cloned.1.call-start = ((), (), s32[]{:S(2)}) async-start(), calls=%async_computation.5 | async-start | bytes 3932160 | tf_op jit(solution)/shard_map/all_gather | solution.py:121
  157.6 3.2 %copy-start.8 = (bf16[1,2048,256]{2,1,0:T(8,128)(2,1)S(1)}, bf16[1,2048,256]{2,1,0:T(8,128)(2,1)}, u32[]{:S(2)}) copy-start(bf16[1,2048,256]{2,1,0:T(8,128)(2,1)} %param.26) | copy-start | bytes 3145732
  160.9 3.0 %copy-start.2 = (bf16[96,2048]{1,0:T(8,128)(2,1)S(1)}, bf16[96,2048]{1,0:T(8,128)(2,1)}, u32[]{:S(2)}) copy-start(bf16[96,2048]{1,0:T(8,128)(2,1)} %param.14) | copy-start | bytes 1179652
  160.9 3.2 %copy-start.6 = (f32[2048]{0:T(1024)S(1)}, f32[2048]{0:T(1024)}, u32[]{:S(2)}) copy-start(f32[2048]{0:T(1024)} %param.16) | copy-start | bytes 24580
  165.6 32.4 %all-to-all-start = ((bf16[4,96,2048]{2,1,0:T(8,128)(2,1)}), bf16[4,96,2048]{2,1,0:T(8,128)(2,1)}, u32[]{:S(2)}, u32[]{:S(2)}) async-start(bf16[4,96,2048]{2,1,0:T(8,128)(2,1)} %broadcast_in_dim.8), calls=%async_computation | async-start | bytes 3145728 | tf_op jit(solution)/shard_map/all_to_all | solution.py:11
  198.0 2.6 copy-start.7
  203.0 6.0 %collective-permute-start = (bf16[2,512]{1,0:T(2,128)(2,1)S(1)}, bf16[2,512]{1,0:T(2,128)(2,1)S(1)}, u32[]{:S(2)}, u32[]{:S(2)}) collective-permute-start(bf16[2,512]{1,0:T(2,128)(2,1)S(1)} %slice.44), channel_id=1, source_target_pairs={{0,4},{4,8},{8,12},{12,16},{16,20},{20,24},{24,28},{28,32},{32,36}... | collective-permute-start | bytes 6152 | tf_op jit(solution)/shard_map/ppermute | solution.py:28
  223.0 51.5 %all-to-all-start.2 = ((bf16[64,24,512]{2,1,0:T(8,128)(2,1)}), bf16[64,24,512]{2,1,0:T(8,128)(2,1)}, u32[]{:S(2)}, u32[]{:S(2)}) async-start(bf16[64,24,512]{2,1,0:T(8,128)(2,1)} %bitcast.45), calls=%async_computation.2 | async-start | bytes 3145728 | tf_op jit(solution)/shard_map/all_to_all | solution.py:127
  235.5 33.1 %all-gather.4.cloned.1.call-start = ((), (), s32[]{:S(2)}) async-start(), calls=%async_computation.3 | async-start | bytes 1966080 | tf_op jit(solution)/shard_map/all_gather | solution.py:115
  235.7 4.2 %copy-start.4 = (f32[384,2]{0,1:T(2,128)S(1)}, f32[384,2]{0,1:T(2,128)}, u32[]{:S(2)}) copy-start(f32[384,2]{0,1:T(2,128)} %param.24) | copy-start | bytes 9220
Sparse Core Ops, SparseCore 0:
  85.8 65.5 all-gather.5
  164.0 53.7 all-gather.7
  239.8 28.7 all-gather.3
where the time goes:
time: 292 us
  waiting for transfers between devices  133 us (46%)
  blocking collectives  62.8 us (22%)
  local copies, waits for them, and re-layouts  27.6 us (9%)
  matrix products  24 us (8%)
  starting transfers between devices  22.4 us (8%)
  between operations  14.1 us (5%)
  other arithmetic  8 us (3%)
    all_gather x1, waiting for transfers between devices, on_device(): arrived = lax.all_gather(arrived, 'tp', axis=1, tiled=True)  65.5 us
    all_to_all x1, blocking collectives, on_device(): lax.all_to_all(outgoing, 'ep', split_axis=0, concat_axis=0, tiled=True)  62.8 us
    all_gather x1, waiting for transfers between devices, on_device(): lax.all_gather(gated, 'tp', axis=1, tiled=True)  28.4 us
    all_to_all x1, waiting for transfers between devices, sent_to_all(): lax.all_to_all(jnp.broadcast_to(x[None], (peers, *x.shape)), axis, 0, 0,...  28 us
    all_to_all x1, starting transfers between devices, on_device(): lax.all_to_all(results, 'ep', split_axis=0, concat_axis=0, tiled=True)  12.5 us
    all_gather x1, waiting for transfers between devices, on_device(): lax.all_gather(hidden, 'tp', axis=1, tiled=True)  8.66 us
    all_gather x1, local copies, waits for them, and re-layouts, on_device(): arrived = lax.all_gather(arrived, 'tp', axis=1, tiled=True)  6.23 us
  transfers between devices with their start and end apart: 6, of which 5 were waited for; matrix products, arithmetic and copies ran while one was open for 5% of the time, Pallas kernels for 0%

commit v1 on v0

--- a/solution.py
+++ b/solution.py
@@ -4,6 +4,12 @@
 from jax.sharding import PartitionSpec as P
 
 norm_eps = 1e-06
+
+
+def tiled_gather(x, axis, dim):
+    length = lax.axis_size(axis)
+    repeats = [length if d == dim else 1 for d in range(x.ndim)]
+    return lax.all_to_all(jnp.tile(x, repeats), axis, split_axis=dim, concat_axis=dim, tiled=True)
 
 
 def sent_to_all(x, axis):
@@ -90,7 +96,7 @@
     )
     outgoing = padded_rows[row_table].reshape(experts, slot_cap, expert_normed.shape[1])
     arrived = lax.all_to_all(outgoing, "ep", split_axis=0, concat_axis=0, tiled=True)
-    arrived = lax.all_gather(arrived, "tp", axis=1, tiled=True)
+    arrived = tiled_gather(arrived, "tp", 1)
     chan_width = in_gate_weight.shape[1]
     in_gate = jnp.dot(mixer_rows, in_gate_weight, preferred_element_type=jnp.float32)
     out_gate = jnp.dot(mixer_rows, out_gate_weight, preferred_element_type=jnp.float32)

time: 292 us -> 294 us (level)
  blocking collectives: 62.8 us -> 136 us
  waiting for transfers between devices: 133 us -> 66 us
  local copies, waits for them, and re-layouts: 27.6 us -> 24.5 us
    all_to_all x0 -> x1, blocking collectives: none -> 72.8 us  [tiled_gather(): lax.all_to_all(jnp.tile(x, repeats), axis, split_axis=dim, concat_axis=di...]
    all_gather x1 -> x0, waiting for transfers between devices: 65.5 us -> none  [on_device(): arrived = lax.all_gather(arrived, 'tp', axis=1, tiled=True)]
    all_gather x1 -> x0, local copies, waits for them, and re-layouts: 6.23 us -> none  [on_device(): arrived = lax.all_gather(arrived, 'tp', axis=1, tiled=True)]
    all_to_all x0 -> x1, local copies, waits for them, and re-layouts: none -> 3.45 us  [tiled_gather(): lax.all_to_all(jnp.tile(x, repeats), axis, split_axis=dim, concat_axis=di...]
  transfers between devices with their start and end apart: 6 -> 5, of which waited for: 5 -> 4; matrix products, arithmetic and copies ran while one was open for 5% -> 5% of each run, Pallas kernels for 0% -> 0%
where the time goes in v1:
time: 294 us; the launch traced here: 293 us
  blocking collectives  136 us (46%)
  waiting for transfers between devices  66 us (22%)
  local copies, waits for them, and re-layouts  24.5 us (8%)
  matrix products  22.7 us (8%)
  starting transfers between devices  21.8 us (7%)
  between operations  14.4 us (5%)
  other arithmetic  8 us (3%)
    all_to_all x1, blocking collectives, tiled_gather(): lax.all_to_all(jnp.tile(x, repeats), axis, split_axis=dim, concat_axis=di...  72.8 us
    all_to_all x1, blocking collectives, on_device(): lax.all_to_all(outgoing, 'ep', split_axis=0, concat_axis=0, tiled=True)  62.8 us
    all_gather x1, waiting for transfers between devices, on_device(): lax.all_gather(gated, 'tp', axis=1, tiled=True)  27.9 us
    all_to_all x1, waiting for transfers between devices, sent_to_all(): lax.all_to_all(jnp.broadcast_to(x[None], (peers, *x.shape)), axis, 0, 0,...  26 us
    all_to_all x1, starting transfers between devices, on_device(): lax.all_to_all(results, 'ep', split_axis=0, concat_axis=0, tiled=True)  10.1 us
    all_gather x1, waiting for transfers between devices, on_device(): lax.all_gather(hidden, 'tp', axis=1, tiled=True)  9.57 us
    ppermute x1, starting transfers between devices, passed_along(): lax.ppermute(value, axis, [(source, source + steps) for source in range(l...  7.02 us
  transfers between devices with their start and end apart: 5, of which 4 were waited for; matrix products, arithmetic and copies ran while one was open for 5% of the time, Pallas kernels for 0%

profile of v1, /device:TPU:1, one launch (start us, length us, event | category | flops | bytes accessed | tf_op | source)
XLA Modules:
  0.0 293.1 jit_solution(2805148648448951049)
XLA Ops:
  7.2 1.0 copy.38
  8.5 2.4 reduce-window.6
  12.3 1.2 scatter_custom_fusion
  13.6 0.2 fusion.10
  14.0 3.1 %gather_fusion = bf16[384,2048]{1,0:T(8,128)(2,1)} fusion(bf16[97,2048]{1,0:T(8,128)(2,1)S(1)} %concatenate.7, s32[1024]{0:T(1024)S(1)} %pad_clamp_fusion.1), kind=kCustom, calls=%fused_computation | custom fusion | bytes 3147264 | tf_op jit(solution)/shard_map/gather | solution.py:97
  17.1 3.7 %reshape.137 = bf16[64,6,2048]{2,1,0:T(8,128)(2,1)} reshape(bf16[384,2048]{1,0:T(8,128)(2,1)} %gather_fusion) | data formatting | bytes 3145728 | tf_op jit(solution)/shard_map/reshape | solution.py:97
  20.8 62.8 %all_to_all.20 = bf16[64,6,2048]{2,1,0:T(8,128)(2,1)S(1)} all-to-all(bf16[64,6,2048]{2,1,0:T(8,128)(2,1)} %reshape.137), channel_id=1, replica_groups=mesh['ep'=64,'tp'=4] {'ep'}, dimensions={0} | all-to-all | bytes 3145728 | tf_op jit(solution)/shard_map/all_to_all | solution.py:98
  83.6 0.9 copy.45
  84.5 0.8 tile.4
  85.3 72.8 %all_to_all.21 = bf16[64,24,2048]{2,0,1:T(8,128)(2,1)S(1)} all-to-all(bf16[64,24,2048]{2,0,1:T(8,128)(2,1)S(1)} %bitcast.44), channel_id=1, replica_groups=mesh['ep'=64,'tp'=4] {'tp'}, dimensions={1} | all-to-all | bytes 12582912 | tf_op jit(solution)/shard_map/all_to_all | solution.py:12
  158.1 3.4 %copy.46 = bf16[64,24,2048]{2,1,0:T(8,128)(2,1)S(1)} copy(bf16[64,24,2048]{2,0,1:T(8,128)(2,1)S(1)} %all_to_all.21) | data formatting | bytes 12582912 | tf_op jit(solution)/shard_map/all_to_all | solution.py:12
  161.6 1.9 fusion.5
  163.5 3.0 %fusion = bf16[1536,256]{1,0:T(8,128)(2,1)} fusion(bf16[1536,2048]{1,0:T(8,128)(2,1)S(1)} %bitcast.46, f32[1536,256]{1,0:T(8,128)S(1)} %fusion.5, bf16[1,2048,256]{2,1,0:T(8,128)(2,1)S(1)} %copy-done.9), kind=kOutput, calls=%fused_computation.5 | convolution fusion | flops 1612972032 | bytes 9699328 | tf_op jit(solution)/shard_map/dot_general | solution.py:116
  166.5 0.2 fusion.7
  166.9 1.4 broadcast_in_dim.8
  168.2 4.3 %all-to-all-start = ((bf16[4,96,2048]{2,1,0:T(8,128)(2,1)}), bf16[4,96,2048]{2,1,0:T(8,128)(2,1)}, u32[]{:S(2)}, u32[]{:S(2)}) async-start(bf16[4,96,2048]{2,1,0:T(8,128)(2,1)} %broadcast_in_dim.8), calls=%async_computation | async-start | bytes 3145728 | tf_op jit(solution)/shard_map/all_to_all | solution.py:17
  172.6 26.0 %all-to-all-done = bf16[4,96,2048]{2,1,0:T(8,128)(2,1)} async-done(((bf16[4,96,2048]{2,1,0:T(8,128)(2,1)}), bf16[4,96,2048]{2,1,0:T(8,128)(2,1)}, u32[]{:S(2)}, u32[]{:S(2)}) %all-to-all-start) | async-done | bytes 1572896 | tf_op jit(solution)/shard_map/all_to_all | solution.py:17
  198.6 2.6 fusion.22
  201.1 2.4 fusion.2
  203.6 7.0 %collective-permute-start = (bf16[2,512]{1,0:T(2,128)(2,1)S(1)}, bf16[2,512]{1,0:T(2,128)(2,1)S(1)}, u32[]{:S(2)}, u32[]{:S(2)}) collective-permute-start(bf16[2,512]{1,0:T(2,128)(2,1)S(1)} %slice.44), channel_id=1, source_target_pairs={{0,4},{4,8},{8,12},{12,16},{16,20},{20,24},{24,28},{28,32},{32,36}... | collective-permute-start | bytes 6152 | tf_op jit(solution)/shard_map/ppermute | solution.py:34
  210.6 0.9 constant_dynamic-slice_fusion
  211.6 9.6 %all-gather.5.cloned.1.call-done = bf16[1536,1024]{1,0:T(8,128)(2,1)} async-done(((bf16[1536,256]{1,0:T(8,128)(2,1)}), bf16[1536,1024]{1,0:T(8,128)(2,1)}) %all-gather.5.cloned.1.call-update) | async-done | bytes 3145744 | tf_op jit(solution)/shard_map/all_gather | solution.py:127
  221.2 5.1 %convolution_convert_fusion = bf16[1536,512]{1,0:T(8,128)(2,1)} fusion(bf16[1536,1024]{1,0:T(8,128)(2,1)} %all-gather.5.cloned.1.call-done, bf16[1,1024,512]{2,1,0:T(8,128)(2,1)} %param.27), kind=kOutput, calls=%fused_computation.3 | convolution fusion | flops 1611399168 | bytes 5767168 | tf_op jit(solution)/shard_map/dot_general | solution.py:126
  226.3 10.1 %all-to-all-start.3 = ((bf16[64,24,512]{2,1,0:T(8,128)(2,1)}), bf16[64,24,512]{2,1,0:T(8,128)(2,1)}, u32[]{:S(2)}, u32[]{:S(2)}) async-start(bf16[64,24,512]{2,1,0:T(8,128)(2,1)} %bitcast.47), calls=%async_computation.3 | async-start | bytes 3145728 | tf_op jit(solution)/shard_map/all_to_all | solution.py:133
  236.5 0.3 all-gather.3.cloned.1.call-start
  236.8 3.9 %fusion.1 = bf16[384,512]{1,0:T(8,128)(2,1)} fusion(bf16[384,2048]{1,0:T(8,128)(2,1)} %bitcast, bf16[2048,512]{1,0:T(8,128)(2,1)} %param.18, f32[386,512]{1,0:T(8,128)S(1)} %maximum_convert_fusion, f32[512]{0:T(512)S(1)} %bitcast.50, f32[512]{0:T(512)S(1)} %bitcast.49, f32[512]{0:T(512)S(1)} %bitcast.48), kind=kOutput, calls=%fused_computation.9 | convolution fusion | flops 806682624 | bytes 6428672 | tf_op jit(solution)/shard_map/dot_general | solution.py:102
  241.2 27.9 %all-gather.3.cloned.1.call-done = bf16[384,2048]{1,0:T(8,128)(2,1)} async-done(((bf16[384,512]{1,0:T(8,128)(2,1)}), bf16[384,2048]{1,0:T(8,128)(2,1)}) %all-gather.3.cloned.1.call-update) | async-done | bytes 1572880 | tf_op jit(solution)/shard_map/all_gather | solution.py:121
  269.1 3.8 %convolution_convert_fusion.1 = bf16[384,512]{1,0:T(8,128)(2,1)} fusion(bf16[384,2048]{1,0:T(8,128)(2,1)} %all-gather.3.cloned.1.call-done, bf16[2048,512]{1,0:T(8,128)(2,1)} %param.21), kind=kOutput, calls=%fused_computation.11 | convolution fusion | flops 805502976 | bytes 4063232 | tf_op jit(solution)/shard_map/dot_general | solution.py:120
  272.9 2.6 all-to-all-done.3
  275.5 4.3 %gather_fusion.1 = bf16[768,512]{1,0:T(8,128)(2,1)S(1)} fusion(bf16[1536,512]{1,0:T(8,128)(2,1)} %bitcast.13, s32[1024]{0:T(1024)S(1)} %pad_clamp_fusion), kind=kCustom, calls=%fused_computation.1 | custom fusion | bytes 1575936 | tf_op jit(solution)/shard_map/gather | solution.py:135
  279.8 2.1 reshape.143
  281.9 4.3 %multiply_reduce_fusion = bf16[384,512]{1,0:T(8,128)(2,1)} fusion(f32[384,2,512]{2,1,0:T(2,128)} %reshape.143, f32[384,2]{1,0:T(8,128)S(1)} %copy.48), kind=kLoop, calls=%fused_computation.6 | loop fusion | flops 589824 | bytes 1969152 | tf_op jit(solution)/shard_map/reduce_sum | solution.py:139
  (62 shorter events, 2.7 us)
Async XLA Ops:
  7.2 191.4 %copy-start = (bf16[2048,512]{1,0:T(8,128)(2,1)S(1)}, bf16[2048,512]{1,0:T(8,128)(2,1)}, u32[]{:S(2)}) copy-start(bf16[2048,512]{1,0:T(8,128)(2,1)} %param.17) | copy-start | bytes 6291460
  7.2 214.0 %all-gather.5.cloned.1.call-start = ((), (), s32[]{:S(2)}) async-start(), calls=%async_computation.5 | async-start | bytes 3932160 | tf_op jit(solution)/shard_map/all_gather | solution.py:127
  8.2 3.6 %copy-start.3 = (s32[384,2]{0,1:T(2,128)S(1)}, s32[384,2]{0,1:T(2,128)}, u32[]{:S(2)}) copy-start(s32[384,2]{0,1:T(2,128)} %param.23) | copy-start | bytes 9220
  8.4 5.1 %copy-start.1 = (bf16[96,2048]{1,0:T(8,128)(2,1)S(1)}, bf16[96,2048]{1,0:T(8,128)(2,1)}, u32[]{:S(2)}) copy-start(bf16[96,2048]{1,0:T(8,128)(2,1)} %param.15) | copy-start | bytes 1179652
  8.4 5.3 %copy-start.5 = (f32[2048]{0:T(1024)S(1)}, f32[2048]{0:T(1024)}, u32[]{:S(2)}) copy-start(f32[2048]{0:T(1024)} %param.22) | copy-start | bytes 24580
  158.1 3.5 %copy-start.8 = (bf16[1,2048,256]{2,1,0:T(8,128)(2,1)S(1)}, bf16[1,2048,256]{2,1,0:T(8,128)(2,1)}, u32[]{:S(2)}) copy-start(bf16[1,2048,256]{2,1,0:T(8,128)(2,1)} %param.25) | copy-start | bytes 3145732
  161.6 1.9 copy-start.9
  163.5 3.0 %copy-start.2 = (bf16[96,2048]{1,0:T(8,128)(2,1)S(1)}, bf16[96,2048]{1,0:T(8,128)(2,1)}, u32[]{:S(2)}) copy-start(bf16[96,2048]{1,0:T(8,128)(2,1)} %param.14) | copy-start | bytes 1179652
  163.5 3.2 %copy-start.6 = (f32[2048]{0:T(1024)S(1)}, f32[2048]{0:T(1024)}, u32[]{:S(2)}) copy-start(f32[2048]{0:T(1024)} %param.16) | copy-start | bytes 24580
  168.2 30.3 %all-to-all-start = ((bf16[4,96,2048]{2,1,0:T(8,128)(2,1)}), bf16[4,96,2048]{2,1,0:T(8,128)(2,1)}, u32[]{:S(2)}, u32[]{:S(2)}) async-start(bf16[4,96,2048]{2,1,0:T(8,128)(2,1)} %broadcast_in_dim.8), calls=%async_computation | async-start | bytes 3145728 | tf_op jit(solution)/shard_map/all_to_all | solution.py:17
  198.6 2.6 copy-start.7
  203.6 7.9 %collective-permute-start = (bf16[2,512]{1,0:T(2,128)(2,1)S(1)}, bf16[2,512]{1,0:T(2,128)(2,1)S(1)}, u32[]{:S(2)}, u32[]{:S(2)}) collective-permute-start(bf16[2,512]{1,0:T(2,128)(2,1)S(1)} %slice.44), channel_id=1, source_target_pairs={{0,4},{4,8},{8,12},{12,16},{16,20},{20,24},{24,28},{28,32},{32,36}... | collective-permute-start | bytes 6152 | tf_op jit(solution)/shard_map/ppermute | solution.py:34
  226.3 49.2 %all-to-all-start.3 = ((bf16[64,24,512]{2,1,0:T(8,128)(2,1)}), bf16[64,24,512]{2,1,0:T(8,128)(2,1)}, u32[]{:S(2)}, u32[]{:S(2)}) async-start(bf16[64,24,512]{2,1,0:T(8,128)(2,1)} %bitcast.47), calls=%async_computation.3 | async-start | bytes 3145728 | tf_op jit(solution)/shard_map/all_to_all | solution.py:133
  236.5 32.6 %all-gather.3.cloned.1.call-start = ((), (), s32[]{:S(2)}) async-start(), calls=%async_computation.4 | async-start | bytes 1966080 | tf_op jit(solution)/shard_map/all_gather | solution.py:121
  236.8 4.2 %copy-start.4 = (f32[384,2]{0,1:T(2,128)S(1)}, f32[384,2]{0,1:T(2,128)}, u32[]{:S(2)}) copy-start(f32[384,2]{0,1:T(2,128)} %param.24) | copy-start | bytes 9220
Sparse Core Ops, SparseCore 0:
  166.6 54.5 all-gather.4
  240.8 28.2 all-gather.2
